TPU v7x, 32 devices: a whole 2x2x4 slice. The times are simulated.
32 devices in a mesh: ep: 8 (over z, x), tp: 4 (over y, core).
Axes of the slice: x: 2, y: 2, z: 4, core: 2. Of those that a mesh axis runs over, the one named last changes fastest.
Arguments:
- tokens: bfloat16 [384, 2048], P('ep', 'tp'), may hold values from -6 to 6
- conv_state: bfloat16 [384, 3, 1024], P('ep', None, 'tp'), may hold values from -6 to 6
- lru_state: float32 [384, 1024], P('ep', 'tp'), may hold values from -6 to 6
- mix_gain: float32 [2048], replicated, may hold values from 0.1 to 1.9
- input_weight: bfloat16 [2048, 1024], P(None, 'tp'), may hold values from -0.125 to 0.125
- branch_weight: bfloat16 [2048, 1024], P(None, 'tp'), may hold values from -0.125 to 0.125
- conv_taps: float32 [4, 1024], P(None, 'tp'), may hold values from -3 to 3
- conv_bias: float32 [1024], P('tp'), may hold values from -3 to 3
- recur_weight: bfloat16 [8, 128, 128], P('tp'), may hold values from -0.5 to 0.5
- recur_bias: float32 [1024], P('tp'), may hold values from -4 to 4
- inject_weight: bfloat16 [8, 128, 128], P('tp'), may hold values from -0.5 to 0.5
- inject_bias: float32 [1024], P('tp'), may hold values from -4 to 4
- decay_param: float32 [1024], P('tp'), may hold values from -1 to 4
- output_weight: bfloat16 [1024, 2048], P(None, 'tp'), may hold values from -0.1875 to 0.1875
- moe_gain: float32 [2048], replicated, may hold values from 0.1 to 1.9
- route_ids: int32 [384, 2], P('ep'), may hold values from 0 to 7, as said below
- route_logits: float32 [384, 2], P('ep'), may hold values from -6 to 6
- group_weight: float32 [384], P('ep'), may hold values from 0.25 to 1
- expert_gate: bfloat16 [8, 2048, 512], P('ep', None, 'tp'), may hold values from -0.125 to 0.125
- expert_up: bfloat16 [8, 2048, 512], P('ep', None, 'tp'), may hold values from -0.125 to 0.125
- expert_down: bfloat16 [8, 512, 2048], P('ep', 'tp'), may hold values from -0.25 to 0.25
Outputs:
- result: bfloat16 [384, 2048], P('ep', 'tp')
- new_state: float32 [384, 1024], P('ep', 'tp')
- new_conv: bfloat16 [384, 3, 1024], P('ep', None, 'tp')
Inputs may be any that keep to these rules, and one draw needn't show every extreme that they name: `route_ids`: each row names 2 different experts of one group of 4 consecutive experts (the group of expert e is e // 4). In each aligned block of 48 rows no expert is named by more than 23 rows, and in every draw some expert is named by exactly 23 rows of every block.
All inputs are finite; a program needn't handle non-finite values.
Results may differ from a plain program's by a relative error of at most 0.013.
Values may be sent and summed in bfloat16 or wider, within the bound.
A program may use at most 64 MiB of HBM per device.

v0:
```python
import jax
import jax.numpy as jnp
from jax import lax
from jax.sharding import PartitionSpec as P

PER_GROUP = 4


EPS = 1e-06
RATE = 8.0


def rms_norm(values, scales):
    wide = values.astype(jnp.float32)
    return wide * lax.rsqrt(jnp.mean(wide * wide, axis=-1, keepdims=True) + EPS) * scales


def block_gate(signal, weight, bias):
    blocks = weight.shape[0]
    grouped = signal.reshape(signal.shape[0], blocks, -1)
    mixed_out = jnp.einsum("sbi,bij->sbj", grouped, weight, preferred_element_type=jnp.float32)
    return jax.nn.sigmoid(mixed_out.reshape(signal.shape[0], -1) + bias)


def body(
    tokens,
    conv_state,
    lru_state,
    mix_gain,
    input_weight,
    branch_weight,
    conv_taps,
    conv_bias,
    recur_weight,
    recur_bias,
    inject_weight,
    inject_bias,
    decay_param,
    output_weight,
    moe_gain,
    route_ids,
    route_logits,
    group_weight,
    expert_gate,
    expert_up,
    expert_down,
):
    seq_count = tokens.shape[0]
    quarter = tokens.shape[1]
    member = lax.axis_index("tp")
    full_tokens = lax.all_gather(tokens, "tp", axis=1, tiled=True)
    model_width = full_tokens.shape[1]
    normed = rms_norm(full_tokens, mix_gain).astype(jnp.bfloat16)
    branch_x = jnp.dot(normed, input_weight, preferred_element_type=jnp.float32).astype(
        jnp.bfloat16
    )
    branch_g = jnp.dot(normed, branch_weight, preferred_element_type=jnp.float32).astype(
        jnp.bfloat16
    )
    window = jnp.concatenate([conv_state, branch_x[:, None, :]], axis=1)
    conv_sum = conv_bias + jnp.sum(window.astype(jnp.float32) * conv_taps[None], axis=1)
    conv_out = conv_sum.astype(jnp.bfloat16)
    recur_gate = block_gate(conv_out, recur_weight, recur_bias)
    inject_gate = block_gate(conv_out, inject_weight, inject_bias)
    log_rate = -RATE * recur_gate * jax.nn.softplus(-decay_param)
    new_state = jnp.exp(log_rate) * lru_state + jnp.sqrt(
        -jnp.expm1(2.0 * log_rate)
    ) * inject_gate * conv_out.astype(jnp.float32)
    mixer_out = (new_state * jax.nn.gelu(branch_g.astype(jnp.float32))).astype(jnp.bfloat16)
    mixed_out = jnp.dot(
        lax.all_gather(mixer_out, "tp", axis=1, tiled=True),
        output_weight,
        preferred_element_type=jnp.float32,
    )
    stream = (tokens.astype(jnp.float32) + mixed_out).astype(jnp.bfloat16)
    top_count = route_ids.shape[1]
    experts = lax.axis_size("ep")
    capacity = max(
        2, min((seq_count - 2) * top_count // PER_GROUP, 2 * seq_count * top_count // experts)
    )
    flat_ids = route_ids.reshape(-1)
    one_hot = (flat_ids[:, None] == jnp.arange(experts, dtype=jnp.int32)[None, :]).astype(jnp.int32)
    earlier = jnp.cumsum(one_hot, axis=0) - one_hot
    slot_rank = jnp.sum(one_hot * earlier, axis=1).reshape(seq_count, top_count)
    slot_index = route_ids * capacity + slot_rank
    targets = jnp.arange(experts * capacity, dtype=jnp.int32)
    dispatch = jnp.sum(
        (targets[:, None, None] == slot_index[None]).astype(jnp.float32), axis=2
    ).astype(jnp.bfloat16)
    raised = jnp.exp(route_logits)
    route_weight = group_weight[:, None] * raised / jnp.sum(raised, axis=1, keepdims=True)
    stream_wide = stream.astype(jnp.float32)
    squares = jnp.sum(stream_wide * stream_wide, axis=1)
    total_sq = lax.psum(squares, "tp")
    gain_part = lax.dynamic_slice_in_dim(moe_gain, member * quarter, quarter, 0)
    moe_part = (stream_wide * lax.rsqrt(total_sq / model_width + EPS)[:, None] * gain_part).astype(
        jnp.bfloat16
    )
    outgoing = jnp.dot(dispatch, moe_part, preferred_element_type=jnp.float32).astype(jnp.bfloat16)
    outgoing = outgoing.reshape(experts, capacity, quarter)
    arrived = lax.all_gather(
        lax.all_to_all(outgoing, "ep", split_axis=0, concat_axis=0, tiled=True),
        "tp",
        axis=2,
        tiled=True,
    )
    senders, slot_count, unused = arrived.shape
    flat_rows = arrived.reshape(senders * slot_count, model_width)
    gate_act = jnp.dot(flat_rows, expert_gate[0], preferred_element_type=jnp.float32)
    up_act = jnp.dot(flat_rows, expert_up[0], preferred_element_type=jnp.float32)
    hidden = (jax.nn.silu(gate_act) * up_act).astype(jnp.bfloat16)
    partial_value = jnp.dot(hidden, expert_down[0], preferred_element_type=jnp.float32)
    partial_value = partial_value.reshape(senders, slot_count, model_width)
    summed = lax.psum_scatter(
        partial_value.astype(jnp.bfloat16), "tp", scatter_dimension=2, tiled=True
    )
    returned = lax.all_to_all(summed, "ep", split_axis=0, concat_axis=0, tiled=True)
    flat_back = returned.reshape(experts * capacity, quarter)
    picked = jnp.take(flat_back, slot_index, axis=0).astype(jnp.float32)
    routed = jnp.sum(route_weight[:, :, None] * picked, axis=1)
    result = (stream.astype(jnp.float32) + routed).astype(jnp.bfloat16)
    return (result, new_state, window[:, 1:])


def solution(mesh):
    in_specs = (
        P("ep", "tp"),
        P("ep", None, "tp"),
        P("ep", "tp"),
        P(),
        P(None, "tp"),
        P(None, "tp"),
        P(None, "tp"),
        P("tp"),
        P("tp", None, None),
        P("tp"),
        P("tp", None, None),
        P("tp"),
        P("tp"),
        P(None, "tp"),
        P(),
        P("ep", None),
        P("ep", None),
        P("ep"),
        P("ep", None, "tp"),
        P("ep", None, "tp"),
        P("ep", "tp", None),
    )
    out_specs = (P("ep", "tp"), P("ep", "tp"), P("ep", None, "tp"))
    return jax.shard_map(body, mesh=mesh, in_specs=in_specs, out_specs=out_specs, check_vma=False)
```

profile of v0, /device:TPU:0, one launch (start us, length us, event | category | flops | bytes accessed | tf_op | source)
XLA Modules:
  0.0 100.6 jit_solution(4721863903514791036)
XLA Ops:
  7.2 0.0 copy-start
  7.2 0.0 copy-start.4
  7.2 0.0 copy-start.12
  7.2 0.0 copy-start.11
  7.2 0.0 copy-start.7
  7.2 0.0 copy-start.8
  7.2 0.0 reduce-scatter.2.cloned.1.call-start
  7.3 0.0 copy-start.17
  7.3 0.0 copy-start.9
  7.3 0.0 copy-start.14
  7.3 0.0 copy-start.15
  7.3 7.2 %all_gather.9 = bf16[48,2048]{1,0:T(8,128)(2,1)S(1)} all-gather(bf16[48,512]{1,0:T(8,128)(2,1)} %param.21), channel_id=1, replica_groups=mesh['ep'=8,'tp'=4] {'tp'}, dimensions={1}, use_global_device_ids=true | all-gather | bytes 245760 | tf_op jit(solution)/shard_map/all_gather | solution.py:51
  14.6 0.1 fusion.9
  14.7 0.0 copy-start.10
  14.7 1.7 %fusion.4 = bf16[48,1,256]{2,0,1:T(8,128)(2,1)S(1)} fusion(bf16[2048,256]{1,0:T(8,128)(2,1)} %param.25, bf16[48,2048]{1,0:T(8,128)(2,1)S(1)} %all_gather.9, f32[2048]{0:T(1024)} %param.24, f32[48]{0:T(128)S(1)} %add_rsqrt_fusion.1), kind=kOutput, calls=%fused_computation.13 | convolution fusion | flops 50737152 | bytes 1278144 | tf_op jit(solution)/shard_map/dot_general | solution.py:54
  16.4 0.0 copy-done.4
  16.5 0.0 copy-start.5
  16.5 0.1 convolution_bitcast_fusion
  16.6 0.1 convolution_bitcast_fusion.1
  16.8 0.0 copy-done.9
  16.8 0.0 copy-done.14
  16.8 0.0 copy-done.15
  16.8 0.1 fusion.36
  16.9 0.0 copy-start.6
  17.0 0.0 copy-start.13
  17.0 0.3 fusion.27
  17.3 5.3 %all_gather.10 = bf16[48,1024]{1,0:T(8,128)(2,1)S(1)} all-gather(bf16[48,256]{1,0:T(8,128)(2,1)S(1)} %fusion.27), channel_id=1, replica_groups=mesh['ep'=8,'tp'=4] {'tp'}, dimensions={1}, use_global_device_ids=true | all-gather | bytes 122880 | tf_op jit(solution)/shard_map/all_gather | solution.py:71
  22.7 0.4 multiply_reduce_fusion.2
  23.1 7.3 %psum.7 = f32[48]{0:T(128)S(1)} all-reduce(f32[48]{0:T(128)S(1)} %get-tuple-element.5), channel_id=1, replica_groups=mesh['ep'=8,'tp'=4] {'tp'}, use_global_device_ids=true, to_apply=%region_7.8 | all-reduce | flops 48 | bytes 384 | tf_op jit(solution)/shard_map/psum | solution.py:94
  30.4 0.1 copy.48
  30.5 0.1 eq.28
  30.6 0.1 fusion.45
  30.7 0.1 reduce_window_sum.11
  30.8 0.2 select_reduce_fusion
  31.0 0.1 reshape.62
  31.1 0.1 copy.49
  31.2 0.1 convert_reduce_fusion
  31.3 0.8 dynamic_slice.3
  32.1 0.3 convolution_convert_fusion.1
  32.3 0.1 reshape.63
  32.4 13.4 %all_to_all.10 = bf16[8,23,512]{2,1,0:T(8,128)(2,1)S(1)} all-to-all(bf16[8,23,512]{2,1,0:T(8,128)(2,1)S(1)} %reshape.63), channel_id=1, replica_groups=mesh['ep'=8,'tp'=4] {'ep'}, dimensions={0} | all-to-all | bytes 376832 | tf_op jit(solution)/shard_map/all_to_all | solution.py:102
  45.8 7.7 %all_gather.11 = bf16[8,23,2048]{2,1,0:T(8,128)(2,1)S(1)} all-gather(bf16[8,23,512]{2,1,0:T(8,128)(2,1)S(1)} %all_to_all.10), channel_id=1, replica_groups=mesh['ep'=8,'tp'=4] {'tp'}, dimensions={2}, use_global_device_ids=true | all-gather | bytes 942080 | tf_op jit(solution)/shard_map/all_gather | solution.py:101
  53.5 0.2 reshape.64
  53.8 0.0 copy-start.19
  53.8 0.4 fusion.7
  54.2 0.7 copy-done.19
  54.8 0.4 fusion.2
  55.2 0.6 copy-done.3
  55.9 1.2 %convolution_convert_fusion = bf16[8,23,2048]{2,1,0:T(8,128)(2,1)} fusion(bf16[8,23,128]{2,1,0:T(8,128)(2,1)S(1)} %dot_general.37, bf16[1,128,2048]{2,1,0:T(8,128)(2,1)S(1)} %copy-done.3), kind=kOutput, calls=%fused_computation.1 | convolution fusion | flops 96845824 | bytes 1325056 | tf_op jit(solution)/shard_map/dot_general | solution.py:112
  57.1 0.0 reduce-scatter.2.cloned.1.call-update
  57.1 0.0 copy-done.16
  57.2 0.0 copy-done.18
  57.2 21.4 %reduce-scatter.2.cloned.1.call-done = bf16[8,23,512]{2,1,0:T(8,128)(2,1)} async-done(((bf16[8,23,2048]{2,1,0:T(8,128)(2,1)}), bf16[8,23,512]{2,1,0:T(8,128)(2,1)}) %reduce-scatter.2.cloned.1.call-update) | async-done | bytes 188432 | tf_op jit(solution)/shard_map/reduce_scatter | solution.py:114
  78.6 5.5 %all-to-all-start.1 = ((bf16[8,23,512]{2,1,0:T(8,128)(2,1)}), bf16[8,23,512]{2,1,0:T(8,128)(2,1)S(1)}, u32[]{:S(2)}, u32[]{:S(2)}) async-start(bf16[8,23,512]{2,1,0:T(8,128)(2,1)} %reduce-scatter.2.cloned.1.call-done), calls=%async_computation.2 | async-start | bytes 393216 | tf_op jit(solution)/shard_map/all_to_all | solution.py:117
  84.1 0.1 copy.51
  84.2 0.1 reshape.68
  84.3 0.1 copy.50
  84.4 0.1 copy.47
  84.5 0.6 fusion.12
  85.2 6.7 %all-to-all-done.1 = bf16[8,23,512]{2,1,0:T(8,128)(2,1)S(1)} async-done(((bf16[8,23,512]{2,1,0:T(8,128)(2,1)}), bf16[8,23,512]{2,1,0:T(8,128)(2,1)S(1)}, u32[]{:S(2)}, u32[]{:S(2)}) %all-to-all-start.1) | async-done | bytes 188448 | tf_op jit(solution)/shard_map/all_to_all | solution.py:117
  91.9 0.1 reshape.65
  92.0 0.8 gather_fusion
  92.8 0.4 multiply_reduce_fusion
  93.1 0.6 add_convert_fusion
  (28 shorter events, 0.2 us)
Async XLA Ops:
  7.2 15.5 %copy-start = (bf16[1024,512]{1,0:T(8,128)(2,1)S(1)}, bf16[1024,512]{1,0:T(8,128)(2,1)}, u32[]{:S(2)}) copy-start(bf16[1024,512]{1,0:T(8,128)(2,1)} %param.34) | copy-start | bytes 3145732
  7.2 9.2 %copy-start.4 = (bf16[48,3,256]{2,0,1:T(8,128)(2,1)S(1)}, bf16[48,3,256]{2,0,1:T(8,128)(2,1)}, u32[]{:S(2)}) copy-start(bf16[48,3,256]{2,0,1:T(8,128)(2,1)} %param.22) | copy-start | bytes 221188
  7.2 9.2 %copy-start.12 = (f32[4,256]{1,0:T(4,128)S(1)}, f32[4,256]{1,0:T(4,128)}, u32[]{:S(2)}) copy-start(f32[4,256]{1,0:T(4,128)} %param.27) | copy-start | bytes 12292
  7.2 9.3 %copy-start.11 = (f32[256]{0:T(256)S(1)}, f32[256]{0:T(256)}, u32[]{:S(2)}) copy-start(f32[256]{0:T(256)} %param.28) | copy-start | bytes 3076
  7.2 9.3 %copy-start.7 = (bf16[2,128,128]{2,1,0:T(8,128)(2,1)S(1)}, bf16[2,128,128]{2,1,0:T(8,128)(2,1)}, u32[]{:S(2)}) copy-start(bf16[2,128,128]{2,1,0:T(8,128)(2,1)} %param.31) | copy-start | bytes 196612
  7.2 9.4 %copy-start.8 = (bf16[2,128,128]{2,1,0:T(8,128)(2,1)S(1)}, bf16[2,128,128]{2,1,0:T(8,128)(2,1)}, u32[]{:S(2)}) copy-start(bf16[2,128,128]{2,1,0:T(8,128)(2,1)} %param.29) | copy-start | bytes 196612
  7.2 71.3 %reduce-scatter.2.cloned.1.call-start = ((), (), s32[]{:S(2)}) async-start(), calls=%async_computation.3 | async-start | bytes 983040 | tf_op jit(solution)/shard_map/reduce_scatter | solution.py:114
  7.3 9.5 %copy-start.17 = (f32[256]{0:T(256)S(1)}, f32[256]{0:T(256)}, u32[]{:S(2)}) copy-start(f32[256]{0:T(256)} %param.33) | copy-start | bytes 3076
  7.3 9.5 %copy-start.9 = (f32[48,256]{1,0:T(8,128)S(1)}, f32[48,256]{1,0:T(8,128)}, u32[]{:S(2)}) copy-start(f32[48,256]{1,0:T(8,128)} %param.23) | copy-start | bytes 147460
  7.3 9.5 %copy-start.14 = (f32[256]{0:T(256)S(1)}, f32[256]{0:T(256)}, u32[]{:S(2)}) copy-start(f32[256]{0:T(256)} %param.32) | copy-start | bytes 3076
  7.3 9.5 %copy-start.15 = (f32[256]{0:T(256)S(1)}, f32[256]{0:T(256)}, u32[]{:S(2)}) copy-start(f32[256]{0:T(256)} %param.30) | copy-start | bytes 3076
  14.7 2.2 %copy-start.1 = (bf16[2048,256]{1,0:T(8,128)(2,1)S(1)}, bf16[2048,256]{1,0:T(8,128)(2,1)}, u32[]{:S(2)}) copy-start(bf16[2048,256]{1,0:T(8,128)(2,1)} %param.26) | copy-start | bytes 3145732
  14.7 2.2 %copy-start.10 = (f32[2048]{0:T(1024)S(1)}, f32[2048]{0:T(1024)}, u32[]{:S(2)}) copy-start(f32[2048]{0:T(1024)} %param.24) | copy-start | bytes 24580
  16.5 6.2 %copy-start.5 = (bf16[48,512]{1,0:T(8,128)(2,1)S(1)}, bf16[48,512]{1,0:T(8,128)(2,1)}, u32[]{:S(2)}) copy-start(bf16[48,512]{1,0:T(8,128)(2,1)} %param.21) | copy-start | bytes 147460
  16.9 6.1 %copy-start.6 = (f32[48,256]{1,0:T(8,128)}, f32[48,256]{1,0:T(8,128)S(1)}, u32[]{:S(2)}) copy-start(f32[48,256]{1,0:T(8,128)S(1)} %fusion.36) | copy-start | bytes 147460
  17.0 13.4 %copy-start.13 = (s32[48,2]{0,1:T(2,128)S(1)}, s32[48,2]{0,1:T(2,128)}, u32[]{:S(2)}) copy-start(s32[48,2]{0,1:T(2,128)} %param.36) | copy-start | bytes 1156
  45.8 8.0 %copy-start.2 = (bf16[1,2048,128]{2,1,0:T(8,128)(2,1)S(1)}, bf16[1,2048,128]{2,1,0:T(8,128)(2,1)}, u32[]{:S(2)}) copy-start(bf16[1,2048,128]{2,1,0:T(8,128)(2,1)} %param.39) | copy-start | bytes 1572868
  53.8 1.0 %copy-start.19 = (bf16[1,2048,128]{2,1,0:T(8,128)(2,1)S(1)}, bf16[1,2048,128]{2,1,0:T(8,128)(2,1)}, u32[]{:S(2)}) copy-start(bf16[1,2048,128]{2,1,0:T(8,128)(2,1)} %param.40) | copy-start | bytes 1572868
  54.8 1.0 %copy-start.3 = (bf16[1,128,2048]{2,1,0:T(8,128)(2,1)S(1)}, bf16[1,128,2048]{2,1,0:T(8,128)(2,1)}, u32[]{:S(2)}) copy-start(bf16[1,128,2048]{2,1,0:T(8,128)(2,1)} %param.41) | copy-start | bytes 1572868
  55.9 1.3 %copy-start.16 = (f32[48,2]{0,1:T(2,128)S(1)}, f32[48,2]{0,1:T(2,128)}, u32[]{:S(2)}) copy-start(f32[48,2]{0,1:T(2,128)} %param.37) | copy-start | bytes 1156
  55.9 1.3 %copy-start.18 = (f32[48]{0:T(128)S(1)}, f32[48]{0:T(128)}, u32[]{:S(2)}) copy-start(f32[48]{0:T(128)} %param.38) | copy-start | bytes 580
  78.6 13.3 %all-to-all-start.1 = ((bf16[8,23,512]{2,1,0:T(8,128)(2,1)}), bf16[8,23,512]{2,1,0:T(8,128)(2,1)S(1)}, u32[]{:S(2)}, u32[]{:S(2)}) async-start(bf16[8,23,512]{2,1,0:T(8,128)(2,1)} %reduce-scatter.2.cloned.1.call-done), calls=%async_computation.2 | async-start | bytes 393216 | tf_op jit(solution)/shard_map/all_to_all | solution.py:117
Sparse Core Ops, SparseCore 0:
  57.3 21.2 reduce-scatter.1
where the time goes:
time: 101 us
  blocking collectives  41 us (41%)
  waiting for transfers between devices  28.1 us (28%)
  between operations  14.4 us (14%)
  starting transfers between devices  5.56 us (6%)
  matrix products  4.86 us (5%)
  local copies, waits for them, and re-layouts  4.23 us (4%)
  other arithmetic  2.45 us (2%)
    reduce_scatter x1, waiting for transfers between devices, body(): lax.psum_scatter(partial_value.astype(jnp.bfloat16), 'tp', scatter_dimens...  21.4 us
    all_to_all x1, blocking collectives, body(): lax.all_to_all(outgoing, 'ep', split_axis=0, concat_axis=0, tiled=True)  13.4 us
    all_gather x1, blocking collectives, body(): lax.all_gather(lax.all_to_all(outgoing, 'ep', split_axis=0, concat_axis=0...  7.74 us
    psum x1, blocking collectives, body(): total_sq = lax.psum(squares, 'tp')  7.3 us
    all_gather x1, blocking collectives, body(): full_tokens = lax.all_gather(tokens, 'tp', axis=1, tiled=True)  7.24 us
    all_to_all x1, waiting for transfers between devices, body(): lax.all_to_all(summed, 'ep', split_axis=0, concat_axis=0, tiled=True)  6.72 us
    all_to_all x1, starting transfers between devices, body(): lax.all_to_all(summed, 'ep', split_axis=0, concat_axis=0, tiled=True)  5.52 us
    all_gather x1, blocking collectives, body(): lax.all_gather(mixer_out, 'tp', axis=1, tiled=True)  5.33 us
  transfers between devices with their start and end apart: 2, of which 2 were waited for; matrix products, arithmetic and copies ran while one was open for 1% of the time, Pallas kernels for 0%

commit v1 on v0

v1 whole, which is shorter than its diff:
```python
import functools

import jax
import jax.numpy as jnp
from jax import lax
from jax.experimental import pallas as pl
from jax.experimental.pallas import tpu as pltpu
from jax.sharding import PartitionSpec as P

PER_GROUP = 4
EPS = 1e-06
RATE = 8.0
GROUP = 2
F32 = jnp.float32
BF16 = jnp.bfloat16


def dot(a, b):
    return jnp.dot(a, b, preferred_element_type=F32)


def kernel(
    experts,
    slots,
    tokens,
    conv_pre,
    lru_state,
    mix_gain,
    tap_last,
    recur_weight,
    recur_bias,
    inject_weight,
    inject_bias,
    decay_param,
    moe_gain,
    ids_col,
    ids_row,
    logits,
    group_weight,
    input_hbm,
    branch_hbm,
    output_hbm,
    gate_hbm,
    up_hbm,
    down_hbm,
    result,
    new_state_ref,
    branch_x_ref,
    w_in,
    w_out,
    w_exp,
    w_down,
    tok_all,
    mix_all,
    stream_ref,
    outbox,
    arrived,
    keep_own,
    keep_cross,
    pbox,
    pin,
    xbox,
    xin,
    rbox,
    rin,
    picked,
    w_sem,
    tok_send,
    tok_recv,
    mix_send,
    mix_recv,
    ep_send,
    ep_recv,
    fw_send,
    fw_recv,
    p_send,
    p_recv,
    x_send,
    x_recv,
    r_send,
    r_recv,
):
    e = lax.axis_index("ep")
    t = lax.axis_index("tp")
    rows, quarter = tokens.shape
    width = mix_gain.shape[1]
    chan = lru_state.shape[1]
    chunks = experts // GROUP
    part = t + 1 - 2 * (t % 2)
    cross = (t + 2) % 4
    diag = (part + 2) % 4
    peers = (part, cross, diag)

    def there(member):
        return {"tp": member}

    loads = (
        (input_hbm, w_in.at[:, pl.ds(0, chan)]),
        (branch_hbm, w_in.at[:, pl.ds(chan, chan)]),
        (output_hbm, w_out),
        (gate_hbm, w_exp.at[:, pl.ds(0, gate_hbm.shape[2])]),
        (up_hbm, w_exp.at[:, pl.ds(gate_hbm.shape[2], gate_hbm.shape[2])]),
        (down_hbm, w_down),
    )
    copies = []
    for number, (source, target) in enumerate(loads):
        src = source.at[0] if number >= 3 else source
        copies.append(pltpu.make_async_copy(src, target, w_sem.at[number]))
        copies[-1].start()

    barrier = pltpu.get_barrier_semaphore()
    for member in peers:
        pl.semaphore_signal(barrier, inc=1, device_id=there(member))

    def greet(k, carry):
        pl.semaphore_signal(barrier, inc=1, device_id={"ep": lax.rem(e + k, experts)})
        return carry

    lax.fori_loop(1, experts, greet, 0)
    pl.semaphore_wait(barrier, 3 + experts - 1)

    tok_copies = []
    for number, member in enumerate(peers):
        tok_copies.append(
            pltpu.make_async_remote_copy(
                src_ref=tokens,
                dst_ref=tok_all.at[number],
                send_sem=tok_send.at[number],
                recv_sem=tok_recv.at[number],
                device_id=there(member),
            )
        )
        tok_copies[-1].start()

    first_c, second_c = ids_col[:, 0:1], ids_col[:, 1:2]
    first_r, second_r = ids_row[0:1, :], ids_row[1:2, :]
    row_i = lax.broadcasted_iota(jnp.int32, (rows, rows), 0)
    col_i = lax.broadcasted_iota(jnp.int32, (rows, rows), 1)

    def slot_row(mine):
        same = ((first_c == mine) | (second_c == mine)) & (row_i < col_i)
        rank = jnp.sum(jnp.where(same, 1.0, 0.0), axis=0, keepdims=True)
        return mine * slots + rank.astype(jnp.int32)

    def slot_col(mine):
        same = ((first_r == mine) | (second_r == mine)) & (col_i < row_i)
        rank = jnp.sum(jnp.where(same, 1.0, 0.0), axis=1, keepdims=True)
        return mine * slots + rank.astype(jnp.int32)

    slot_r0, slot_r1 = slot_row(first_r), slot_row(second_r)
    slot_c0, slot_c1 = slot_col(first_c), slot_col(second_c)
    raised = jnp.exp(logits[...])
    route_weight = group_weight[...] * raised / jnp.sum(raised, axis=1, keepdims=True)

    copies[0].wait()
    copies[1].wait()
    total = jnp.zeros((rows, 2 * chan), F32)
    squares = jnp.zeros((rows, 1), F32)
    for number, member in enumerate((t,) + peers):
        if number:
            tok_copies[number - 1].wait_recv()
            wide = tok_all[number - 1].astype(F32)
        else:
            wide = tokens[...].astype(F32)
        span = pl.ds(pl.multiple_of(member * quarter, quarter), quarter)
        squares += jnp.sum(wide * wide, axis=1, keepdims=True)
        total += dot((wide * mix_gain[:, span]).astype(BF16), w_in[span, :])
    total = total * lax.rsqrt(squares / width + EPS)
    branch_x = total[:, :chan].astype(BF16)
    branch_g = total[:, chan:].astype(BF16).astype(F32)
    branch_x_ref[...] = branch_x
    conv_out = (conv_pre[...] + branch_x.astype(F32) * tap_last[...]).astype(BF16)
    block = recur_weight.shape[1]
    recur, inject = [], []
    for b in range(recur_weight.shape[0]):
        piece = conv_out[:, b * block : (b + 1) * block]
        recur.append(dot(piece, recur_weight[b]))
        inject.append(dot(piece, inject_weight[b]))
    recur_gate = jax.nn.sigmoid(jnp.concatenate(recur, axis=1) + recur_bias[...])
    inject_gate = jax.nn.sigmoid(jnp.concatenate(inject, axis=1) + inject_bias[...])
    neg = -decay_param[...]
    soft = jnp.maximum(neg, 0.0) + jnp.log1p(jnp.exp(-jnp.abs(neg)))
    log_rate = -RATE * recur_gate * soft
    new_state = jnp.exp(log_rate) * lru_state[...] + jnp.sqrt(
        1.0 - jnp.exp(2.0 * log_rate)
    ) * inject_gate * conv_out.astype(F32)
    new_state_ref[...] = new_state
    mix_all[0] = (new_state * jax.nn.gelu(branch_g)).astype(BF16)

    mix_copies = []
    for number, member in enumerate(peers):
        mix_copies.append(
            pltpu.make_async_remote_copy(
                src_ref=mix_all.at[0],
                dst_ref=mix_all.at[number + 1],
                send_sem=mix_send.at[number],
                recv_sem=mix_recv.at[number],
                device_id=there(member),
            )
        )
        mix_copies[-1].start()
    target = lax.broadcasted_iota(jnp.int32, (experts * slots, rows), 0)
    dispatch = jnp.where((target == slot_r0) | (target == slot_r1), 1.0, 0.0).astype(BF16)
    copies[2].wait()
    mixed = tokens[...].astype(F32)
    for number, member in enumerate((t,) + peers):
        if number:
            mix_copies[number - 1].wait_recv()
        span = pl.ds(pl.multiple_of(member * chan, chan), chan)
        mixed += dot(mix_all[number], w_out[span, :])
    stream = mixed.astype(BF16)
    stream_ref[...] = stream
    sorted_rows = dot(dispatch, stream)
    for number in range(experts):
        outbox[number] = sorted_rows[number * slots : (number + 1) * slots].astype(BF16)
    arrived[t, 0] = outbox[e]

    def ep_copy(k):
        to = lax.rem(e + k, experts)
        return pltpu.make_async_remote_copy(
            src_ref=outbox.at[to],
            dst_ref=arrived.at[t, k],
            send_sem=ep_send.at[k],
            recv_sem=ep_recv.at[k],
            device_id={"ep": to},
        )

    def ep_start(k, carry):
        ep_copy(k).start()
        return carry

    lax.fori_loop(1, experts, ep_start, 0)

    def forward(kind, j):
        owner = (t, t, cross)[kind]
        member = (part, cross, part)[kind]
        span = pl.ds(j * GROUP, GROUP)
        return pltpu.make_async_remote_copy(
            src_ref=arrived.at[owner, span],
            dst_ref=arrived.at[owner, span],
            send_sem=fw_send.at[kind, j],
            recv_sem=fw_recv.at[kind, j],
            device_id=there(member),
        )

    def spread(j, carry):
        @pl.when(j < chunks)
        def _():
            for g in range(GROUP):
                k = j * GROUP + g

                @pl.when(k > 0)
                def _():
                    ep_copy(k).wait_recv()

            forward(0, j).start()
            forward(1, j).start()

        @pl.when(j > 0)
        def _():
            forward(1, j - 1).wait_recv()
            forward(2, j - 1).start()

        return carry

    lax.fori_loop(0, chunks + 1, spread, 0)

    for number in (3, 4, 5):
        copies[number].wait()
    hidden_width = w_down.shape[0]

    def p_copy(j):
        return pltpu.make_async_remote_copy(
            src_ref=pbox.at[j],
            dst_ref=pin.at[j],
            send_sem=p_send.at[j],
            recv_sem=p_recv.at[j],
            device_id=there(part),
        )

    def x_copy(j):
        return pltpu.make_async_remote_copy(
            src_ref=xbox.at[j],
            dst_ref=xin.at[j],
            send_sem=x_send.at[j],
            recv_sem=x_recv.at[j],
            device_id=there(cross),
        )

    def r_copy(k):
        to = lax.rem(e - k + experts, experts)
        return pltpu.make_async_remote_copy(
            src_ref=rbox.at[k],
            dst_ref=rin.at[k],
            send_sem=r_send.at[k],
            recv_sem=r_recv.at[k],
            device_id={"ep": to},
        )

    def expert(j, carry):
        @pl.when(j < chunks)
        def _():
            forward(0, j).wait_recv()
            forward(2, j).wait_recv()
            act = jnp.zeros((GROUP * slots, 2 * hidden_width), F32)
            sq = jnp.zeros((GROUP * slots, 1), F32)
            for member in range(4):
                wide = jnp.concatenate(
                    [arrived[member, j * GROUP + g].astype(F32) for g in range(GROUP)], axis=0
                )
                span = pl.ds(member * quarter, quarter)
                sq += jnp.sum(wide * wide, axis=1, keepdims=True)
                act += dot((wide * moe_gain[:, span]).astype(BF16), w_exp[span, :])
            act = act * lax.rsqrt(sq / width + EPS)
            hidden = (jax.nn.silu(act[:, :hidden_width]) * act[:, hidden_width:]).astype(BF16)

            def partial_out(member):
                span = pl.ds(pl.multiple_of(member * quarter, quarter), quarter)
                return dot(hidden, w_down[:, span])

            pbox[j, 0] = partial_out(part).astype(BF16)
            pbox[j, 1] = partial_out(diag).astype(BF16)
            p_copy(j).start()
            keep_own[j] = partial_out(t)
            keep_cross[j] = partial_out(cross)

        @pl.when((j > 0) & (j <= chunks))
        def _():
            p_copy(j - 1).wait_recv()
            xbox[j - 1] = (keep_cross[j - 1] + pin[j - 1, 1].astype(F32)).astype(BF16)
            x_copy(j - 1).start()

        @pl.when(j > 1)
        def _():
            x_copy(j - 2).wait_recv()
            done = keep_own[j - 2] + pin[j - 2, 0].astype(F32) + xin[j - 2].astype(F32)
            for g in range(GROUP):
                k = (j - 2) * GROUP + g
                rbox[k] = done[g * slots : (g + 1) * slots].astype(BF16)

                @pl.when(k > 0)
                def _():
                    r_copy(k).start()

        return carry

    lax.fori_loop(0, chunks + 2, expert, 0)

    lane = lax.broadcasted_iota(jnp.int32, (rows, slots), 1)

    def choose(k):
        first = lax.rem(e + k, experts) * slots
        return jnp.concatenate(
            [
                jnp.where(lane + first == slot_c0, 1.0, 0.0),
                jnp.where(lane + first == slot_c1, 1.0, 0.0),
            ],
            axis=0,
        ).astype(BF16)

    picked[...] = dot(choose(0), rbox[0])

    def gather(k, carry):
        r_copy(k).wait_recv()
        picked[...] += dot(choose(k), rin[k])
        return carry

    lax.fori_loop(1, experts, gather, 0)
    result[...] = (
        stream_ref[...].astype(F32)
        + route_weight[:, 0:1] * picked[:rows]
        + route_weight[:, 1:2] * picked[rows:]
    ).astype(BF16)

    for copy in tok_copies + mix_copies:
        copy.wait_send()

    def drain_ep(k, carry):
        ep_copy(k).wait_send()
        r_copy(k).wait_send()
        return carry

    lax.fori_loop(1, experts, drain_ep, 0)

    def drain_tp(j, carry):
        for kind in range(3):
            forward(kind, j).wait_send()
        p_copy(j).wait_send()
        x_copy(j).wait_send()
        return carry

    lax.fori_loop(0, chunks, drain_tp, 0)


def body(
    tokens,
    conv_state,
    lru_state,
    mix_gain,
    input_weight,
    branch_weight,
    conv_taps,
    conv_bias,
    recur_weight,
    recur_bias,
    inject_weight,
    inject_bias,
    decay_param,
    output_weight,
    moe_gain,
    route_ids,
    route_logits,
    group_weight,
    expert_gate,
    expert_up,
    expert_down,
):
    rows, quarter = tokens.shape
    chan = lru_state.shape[1]
    width = mix_gain.shape[0]
    hidden = expert_gate.shape[2]
    top_count = route_ids.shape[1]
    experts = lax.axis_size("ep")
    tp = lax.axis_size("tp")
    capacity = max(2, min((rows - 2) * top_count // PER_GROUP, 2 * rows * top_count // experts))
    slots = -(-capacity // 8) * 8
    chunks = experts // GROUP
    conv_pre = conv_bias + jnp.sum(conv_state.astype(F32) * conv_taps[None, :-1], axis=1)
    vmem = pl.BlockSpec(memory_space=pltpu.VMEM)
    anywhere = pl.BlockSpec(memory_space=pl.ANY)
    dma = pltpu.SemaphoreType.DMA
    result, new_state, branch_x = pl.pallas_call(
        functools.partial(kernel, experts, slots),
        out_shape=(
            jax.ShapeDtypeStruct((rows, quarter), BF16),
            jax.ShapeDtypeStruct((rows, chan), F32),
            jax.ShapeDtypeStruct((rows, chan), BF16),
        ),
        in_specs=[vmem] * 15 + [anywhere] * 6,
        out_specs=(vmem, vmem, vmem),
        scratch_shapes=[
            pltpu.VMEM((width, 2 * chan), BF16),
            pltpu.VMEM((output_weight.shape[0], quarter), BF16),
            pltpu.VMEM((width, 2 * hidden), BF16),
            pltpu.VMEM((hidden, width), BF16),
            pltpu.VMEM((3, rows, quarter), BF16),
            pltpu.VMEM((4, rows, chan), BF16),
            pltpu.VMEM((rows, quarter), BF16),
            pltpu.VMEM((experts, slots, quarter), BF16),
            pltpu.VMEM((tp, experts, slots, quarter), BF16),
            pltpu.VMEM((chunks, GROUP * slots, quarter), F32),
            pltpu.VMEM((chunks, GROUP * slots, quarter), F32),
            pltpu.VMEM((chunks, 2, GROUP * slots, quarter), BF16),
            pltpu.VMEM((chunks, 2, GROUP * slots, quarter), BF16),
            pltpu.VMEM((chunks, GROUP * slots, quarter), BF16),
            pltpu.VMEM((chunks, GROUP * slots, quarter), BF16),
            pltpu.VMEM((experts, slots, quarter), BF16),
            pltpu.VMEM((experts, slots, quarter), BF16),
            pltpu.VMEM((2 * rows, quarter), F32),
            dma((6,)),
            dma((3,)),
            dma((3,)),
            dma((3,)),
            dma((3,)),
            dma((experts,)),
            dma((experts,)),
            dma((3, chunks)),
            dma((3, chunks)),
            dma((chunks,)),
            dma((chunks,)),
            dma((chunks,)),
            dma((chunks,)),
            dma((experts,)),
            dma((experts,)),
        ],
        compiler_params=pltpu.CompilerParams(collective_id=0, has_side_effects=True),
    )(
        tokens,
        conv_pre,
        lru_state,
        mix_gain[None],
        conv_taps[-1:],
        recur_weight,
        recur_bias[None],
        inject_weight,
        inject_bias[None],
        decay_param[None],
        moe_gain[None],
        route_ids,
        route_ids.T,
        route_logits,
        group_weight[:, None],
        input_weight,
        branch_weight,
        output_weight,
        expert_gate,
        expert_up,
        expert_down,
    )
    new_conv = jnp.concatenate([conv_state[:, 1:], branch_x[:, None, :]], axis=1)
    return (result, new_state, new_conv)


def solution(mesh):
    in_specs = (
        P("ep", "tp"),
        P("ep", None, "tp"),
        P("ep", "tp"),
        P(),
        P(None, "tp"),
        P(None, "tp"),
        P(None, "tp"),
        P("tp"),
        P("tp", None, None),
        P("tp"),
        P("tp", None, None),
        P("tp"),
        P("tp"),
        P(None, "tp"),
        P(),
        P("ep", None),
        P("ep", None),
        P("ep"),
        P("ep", None, "tp"),
        P("ep", None, "tp"),
        P("ep", "tp", None),
    )
    out_specs = (P("ep", "tp"), P("ep", "tp"), P("ep", None, "tp"))
    return jax.shard_map(body, mesh=mesh, in_specs=in_specs, out_specs=out_specs, check_vma=False)
```

time: 101 us -> 51.8 us (0.51)
  blocking collectives: 41 us -> 0 us
  Pallas kernels: 0 us -> 40.9 us
  waiting for transfers between devices: 28.1 us -> 0 us
  between operations: 14.4 us -> 0.67 us
  starting transfers between devices: 5.56 us -> 0 us
  matrix products: 4.86 us -> 0 us
  local copies, waits for them, and re-layouts: 4.23 us -> 8.44 us
  other arithmetic: 2.45 us -> 1.28 us
    pallas_call x0 -> x1, Pallas kernels: none -> 40.9 us  [body(): pl.pallas_call(functools.partial(kernel, experts, slots), out_shape=(jax....]
    reduce_scatter x1 -> x0, waiting for transfers between devices: 21.4 us -> none  [body(): lax.psum_scatter(partial_value.astype(jnp.bfloat16), 'tp', scatter_dimens...]
    all_gather x3 -> x0, blocking collectives: 20.3 us -> none  [the longest x1 7.74 us: body(): lax.all_gather(lax.all_to_all(outgoing, 'ep', split_axis=0, concat_axis=0...]
    all_to_all x1 -> x0, blocking collectives: 13.4 us -> none  [body(): lax.all_to_all(outgoing, 'ep', split_axis=0, concat_axis=0, tiled=True)]
    psum x1 -> x0, blocking collectives: 7.3 us -> none  [body(): total_sq = lax.psum(squares, 'tp')]
    all_to_all x1 -> x0, waiting for transfers between devices: 6.72 us -> none  [body(): lax.all_to_all(summed, 'ep', split_axis=0, concat_axis=0, tiled=True)]
    all_to_all x1 -> x0, starting transfers between devices: 5.52 us -> none  [body(): lax.all_to_all(summed, 'ep', split_axis=0, concat_axis=0, tiled=True)]
    dot_general x9 -> x0, matrix products: 4.86 us -> none  [the longest x1 1.66 us: body(): jnp.dot(normed, input_weight, preferred_element_type=jnp.float32)]
  transfers between devices with their start and end apart: 2 -> 0, of which waited for: 2 -> 0; matrix products, arithmetic and copies ran while one was open for 1% -> 0% of each run, Pallas kernels for 0% -> 0%
where the time goes in v1:
time: 51.8 us; the launch traced here: 51.3 us
  Pallas kernels  40.9 us (79%)
  local copies, waits for them, and re-layouts  8.44 us (16%)
  other arithmetic  1.28 us (2%)
  between operations  0.67 us (1%)
    pallas_call x1, Pallas kernels, body(): pl.pallas_call(functools.partial(kernel, experts, slots), out_shape=(jax....  40.9 us
    unnamed x16, local copies, waits for them, and re-layouts  5.02 us
    broadcast_in_dim x1, local copies, waits for them, and re-layouts, body(): group_weight[:, None]  1.34 us
    slice x1, local copies, waits for them, and re-layouts, body(): conv_taps[-1:]  1.3 us

profile of v1, /device:TPU:0, one launch (start us, length us, event | category | flops | bytes accessed | tf_op | source)
XLA Modules:
  0.0 51.3 jit_solution(4032708472549839970)
XLA Ops:
  0.6 0.0 copy-start
  0.6 1.3 %slice.10.tap_last = f32[1,256]{1,0:T(1,128)} slice(f32[4,256]{1,0:T(4,128)} %param.27), slice={[3:4], [0:256]} | slice | bytes 2048 | tf_op jit(solution)/shard_map/slice | solution.py:482
  1.9 1.4 %copy.25.logits = f32[48,2]{1,0:T(8,128)} copy(f32[48,2]{0,1:T(2,128)} %param.37) | data formatting | bytes 768 | tf_op args[16]
  3.3 1.3 %copy.26.group_weight = f32[48,1]{1,0:T(8,128)} copy(f32[48,1]{0,1:T(1,128)} %bitcast.17) | data formatting | bytes 384 | tf_op jit(solution)/shard_map/broadcast_in_dim | solution.py:492
  4.7 0.0 copy-start.4
  4.7 1.4 %copy.24.ids_col = s32[48,2]{1,0:T(8,128)} copy(s32[48,2]{0,1:T(2,128)} %param.36) | data formatting | bytes 768 | tf_op args[15]
  6.0 0.0 copy-done
  6.0 0.0 copy-done.4
  6.0 0.0 copy-start.5
  6.1 0.7 %copy-done.5 = f32[256]{0:T(256)S(1)} copy-done((f32[256]{0:T(256)S(1)}, f32[256]{0:T(256)}, u32[]{:S(2)}) %copy-start.5) | copy-done | bytes 1048
  6.7 0.6 %broadcast_add_fusion.conv_pre = f32[48,256]{1,0:T(8,128)} fusion(f32[48,256]{1,0:T(8,128)S(1)} %multiply_reduce_fusion, f32[256]{0:T(256)S(1)} %copy-done.5), kind=kLoop, calls=%fused_computation.2 | loop fusion | flops 12288 | bytes 99328 | tf_op jit(solution)/shard_map/add | solution.py:428
  7.3 40.9 %shard_map.220 = (bf16[48,512]{1,0:T(8,128)(2,1)}, f32[48,256]{1,0:T(8,128)}, bf16[48,256]{1,0:T(8,128)(2,1)}) custom-call(bf16[48,512]{1,0:T(8,128)(2,1)} %tokens.1, f32[48,256]{1,0:T(8,128)} %broadcast_add_fusion.conv_pre, f32[48,256]{1,0:T(8,128)} %lru_state.1, f32[1,2048]{1,0:T(1,128)} %bitcast.10, f32[1,256]{1,0:T(1,128)} %slice.10.tap_last, ...), custom_call_target="tpu_custom_call" | custom-call | tf_op jit(solution)/shard_map/pallas_call | solution.py:432
  48.3 0.0 slice-start
  48.3 0.0 copy-start.3
  48.3 0.8 %slice-done = bf16[48,2,256]{2,0,1:T(8,128)(2,1)S(1)} async-done(((bf16[48,3,256]{2,0,1:T(8,128)(2,1)}), bf16[48,2,256]{2,0,1:T(8,128)(2,1)S(1)}, s32[]{:S(2)}) %slice-start) | async-done | bytes 49176 | tf_op jit(solution)/shard_map/slice | solution.py:500
  49.1 0.0 copy-done.3
  49.1 0.0 copy-start.2
  49.1 0.6 %pad_maximum_fusion = bf16[48,3,256]{2,0,1:T(8,128)(2,1)} fusion(bf16[48,1,256]{2,0,1:T(8,128)(2,1)S(1)} %bitcast.9, bf16[48,2,256]{2,0,1:T(8,128)(2,1)S(1)} %slice-done), kind=kLoop, calls=%fused_computation.1 | loop fusion | flops 36864 | bytes 147456 | tf_op jit(solution)/shard_map/concatenate | solution.py:500
  49.7 0.2 copy-done.2
  49.9 0.0 copy-start.1
  49.9 0.6 %copy.29 = bf16[48,512]{1,0:T(8,128)(2,1)} copy(bf16[48,512]{1,0:T(8,128)(2,1)S(1)} %copy-done.2) | data formatting | bytes 98304
  50.5 0.2 copy-done.1
  50.7 0.6 %copy.30 = f32[48,256]{1,0:T(8,128)} copy(f32[48,256]{1,0:T(8,128)S(1)} %copy-done.1) | data formatting | bytes 98304
  (1 shorter events, 0.0 us)
Async XLA Ops:
  0.6 5.4 %copy-start = (bf16[48,3,256]{2,0,1:T(8,128)(2,1)S(1)}, bf16[48,3,256]{2,0,1:T(8,128)(2,1)}, u32[]{:S(2)}) copy-start(bf16[48,3,256]{2,0,1:T(8,128)(2,1)} %param.22) | copy-start | bytes 221188
  4.7 1.4 %copy-start.4 = (f32[4,256]{1,0:T(4,128)S(1)}, f32[4,256]{1,0:T(4,128)}, u32[]{:S(2)}) copy-start(f32[4,256]{1,0:T(4,128)} %param.27) | copy-start | bytes 12292
  6.0 0.7 %copy-start.5 = (f32[256]{0:T(256)S(1)}, f32[256]{0:T(256)}, u32[]{:S(2)}) copy-start(f32[256]{0:T(256)} %param.28) | copy-start | bytes 3076
  48.3 0.8 %slice-start = ((bf16[48,3,256]{2,0,1:T(8,128)(2,1)}), bf16[48,2,256]{2,0,1:T(8,128)(2,1)S(1)}, s32[]{:S(2)}) async-start(bf16[48,3,256]{2,0,1:T(8,128)(2,1)} %param.22), calls=%async_computation | async-start | bytes 98304 | tf_op jit(solution)/shard_map/slice | solution.py:500
  48.3 0.8 %copy-start.3 = (bf16[48,256]{1,0:T(8,128)(2,1)S(1)}, bf16[48,256]{1,0:T(8,128)(2,1)}, u32[]{:S(2)}) copy-start(bf16[48,256]{1,0:T(8,128)(2,1)} %get-tuple-element.8) | copy-start | bytes 73732
  49.1 0.8 %copy-start.2 = (bf16[48,512]{1,0:T(8,128)(2,1)S(1)}, bf16[48,512]{1,0:T(8,128)(2,1)}, u32[]{:S(2)}) copy-start(bf16[48,512]{1,0:T(8,128)(2,1)} %get-tuple-element.12) | copy-start | bytes 147460
  49.9 0.8 %copy-start.1 = (f32[48,256]{1,0:T(8,128)S(1)}, f32[48,256]{1,0:T(8,128)}, u32[]{:S(2)}) copy-start(f32[48,256]{1,0:T(8,128)} %get-tuple-element.13) | copy-start | bytes 147460

commit v2 on v1

--- a/solution.py
+++ b/solution.py
@@ -22,64 +22,90 @@
 def kernel(
     experts,
     slots,
-    tokens,
-    conv_pre,
-    lru_state,
-    mix_gain,
-    tap_last,
-    recur_weight,
-    recur_bias,
-    inject_weight,
-    inject_bias,
-    decay_param,
-    moe_gain,
-    ids_col,
-    ids_row,
-    logits,
-    group_weight,
-    input_hbm,
-    branch_hbm,
-    output_hbm,
-    gate_hbm,
-    up_hbm,
-    down_hbm,
-    result,
-    new_state_ref,
-    branch_x_ref,
-    w_in,
-    w_out,
-    w_exp,
-    w_down,
-    tok_all,
-    mix_all,
-    stream_ref,
-    outbox,
-    arrived,
-    keep_own,
-    keep_cross,
-    pbox,
-    pin,
-    xbox,
-    xin,
-    rbox,
-    rin,
-    picked,
-    w_sem,
-    tok_send,
-    tok_recv,
-    mix_send,
-    mix_recv,
-    ep_send,
-    ep_recv,
-    fw_send,
-    fw_recv,
-    p_send,
-    p_recv,
-    x_send,
-    x_recv,
-    r_send,
-    r_recv,
+    *refs,
 ):
+    (
+        tokens_hbm,
+        mix_gain_hbm,
+        ids_hbm,
+        logits_hbm,
+        group_hbm,
+        input_hbm,
+        branch_hbm,
+        conv_hbm,
+        taps_hbm,
+        bias_hbm,
+        recur_hbm,
+        recur_bias_hbm,
+        inject_hbm,
+        inject_bias_hbm,
+        decay_hbm,
+        state_hbm,
+        output_hbm,
+        moe_gain_hbm,
+        gate_hbm,
+        up_hbm,
+        down_hbm,
+        result_hbm,
+        new_state_hbm,
+        new_conv_hbm,
+    ) = refs[:24]
+    (
+        tokens,
+        mix_gain,
+        ids_row,
+        logits,
+        group_weight,
+        conv_state,
+        conv_taps,
+        conv_bias,
+        recur_weight,
+        recur_bias,
+        inject_weight,
+        inject_bias,
+        decay_param,
+        lru_state,
+        moe_gain,
+        result,
+        new_state_ref,
+        new_conv,
+    ) = refs[24:42]
+    (
+        w_in,
+        w_out,
+        w_exp,
+        w_down,
+        tok_all,
+        mix_all,
+        stream_ref,
+        outbox,
+        arrived,
+        keep_own,
+        keep_cross,
+        pbox,
+        pin,
+        xbox,
+        xin,
+        rbox,
+        rin,
+        picked,
+        w_sem,
+        o_sem,
+        tok_send,
+        tok_recv,
+        mix_send,
+        mix_recv,
+        ep_send,
+        ep_recv,
+        fw_send,
+        fw_recv,
+        p_send,
+        p_recv,
+        x_send,
+        x_recv,
+        r_send,
+        r_recv,
+    ) = refs[42:]
     e = lax.axis_index("ep")
     t = lax.axis_index("tp")
     rows, quarter = tokens.shape
@@ -94,18 +120,33 @@
     def there(member):
         return {"tp": member}
 
+    hidden_width = down_hbm.shape[1]
     loads = (
+        (tokens_hbm, tokens),
+        (mix_gain_hbm, mix_gain),
+        (ids_hbm, ids_row),
+        (logits_hbm, logits),
+        (group_hbm, group_weight),
         (input_hbm, w_in.at[:, pl.ds(0, chan)]),
         (branch_hbm, w_in.at[:, pl.ds(chan, chan)]),
+        (conv_hbm, conv_state),
+        (taps_hbm, conv_taps),
+        (bias_hbm, conv_bias),
+        (recur_hbm, recur_weight),
+        (recur_bias_hbm, recur_bias),
+        (inject_hbm, inject_weight),
+        (inject_bias_hbm, inject_bias),
+        (decay_hbm, decay_param),
+        (state_hbm, lru_state),
         (output_hbm, w_out),
-        (gate_hbm, w_exp.at[:, pl.ds(0, gate_hbm.shape[2])]),
-        (up_hbm, w_exp.at[:, pl.ds(gate_hbm.shape[2], gate_hbm.shape[2])]),
-        (down_hbm, w_down),
+        (moe_gain_hbm, moe_gain),
+        (gate_hbm.at[0], w_exp.at[:, pl.ds(0, hidden_width)]),
+        (up_hbm.at[0], w_exp.at[:, pl.ds(hidden_width, hidden_width)]),
+        (down_hbm.at[0], w_down),
     )
     copies = []
     for number, (source, target) in enumerate(loads):
-        src = source.at[0] if number >= 3 else source
-        copies.append(pltpu.make_async_copy(src, target, w_sem.at[number]))
+        copies.append(pltpu.make_async_copy(source, target, w_sem.at[number]))
         copies[-1].start()
 
     barrier = pltpu.get_barrier_semaphore()
@@ -119,6 +160,7 @@
     lax.fori_loop(1, experts, greet, 0)
     pl.semaphore_wait(barrier, 3 + experts - 1)
 
+    copies[0].wait()
     tok_copies = []
     for number, member in enumerate(peers):
         tok_copies.append(
@@ -132,10 +174,17 @@
         )
         tok_copies[-1].start()
 
-    first_c, second_c = ids_col[:, 0:1], ids_col[:, 1:2]
+    for number in (2, 3, 4):
+        copies[number].wait()
     first_r, second_r = ids_row[0:1, :], ids_row[1:2, :]
     row_i = lax.broadcasted_iota(jnp.int32, (rows, rows), 0)
     col_i = lax.broadcasted_iota(jnp.int32, (rows, rows), 1)
+
+    def as_col(row):
+        spread_out = jnp.where(row_i == col_i, row.astype(F32), 0.0)
+        return jnp.sum(spread_out, axis=1, keepdims=True)
+
+    first_c, second_c = as_col(first_r).astype(jnp.int32), as_col(second_r).astype(jnp.int32)
 
     def slot_row(mine):
         same = ((first_c == mine) | (second_c == mine)) & (row_i < col_i)
@@ -150,10 +199,11 @@
     slot_r0, slot_r1 = slot_row(first_r), slot_row(second_r)
     slot_c0, slot_c1 = slot_col(first_c), slot_col(second_c)
     raised = jnp.exp(logits[...])
-    route_weight = group_weight[...] * raised / jnp.sum(raised, axis=1, keepdims=True)
-
-    copies[0].wait()
-    copies[1].wait()
+    weight_row = group_weight[...] * raised / jnp.sum(raised, axis=0, keepdims=True)
+    weight_0, weight_1 = as_col(weight_row[0:1, :]), as_col(weight_row[1:2, :])
+
+    for number in (1, 5, 6):
+        copies[number].wait()
     total = jnp.zeros((rows, 2 * chan), F32)
     squares = jnp.zeros((rows, 1), F32)
     for number, member in enumerate((t,) + peers):
@@ -168,8 +218,16 @@
     total = total * lax.rsqrt(squares / width + EPS)
     branch_x = total[:, :chan].astype(BF16)
     branch_g = total[:, chan:].astype(BF16).astype(F32)
-    branch_x_ref[...] = branch_x
-    conv_out = (conv_pre[...] + branch_x.astype(F32) * tap_last[...]).astype(BF16)
+    for number in range(7, 16):
+        copies[number].wait()
+    taps = conv_taps.shape[0]
+    conv_sum = conv_bias[...] + branch_x.astype(F32) * conv_taps[taps - 1 : taps, :]
+    for tap in range(taps - 1):
+        conv_sum += conv_state[tap].astype(F32) * conv_taps[tap : tap + 1, :]
+    conv_out = conv_sum.astype(BF16)
+    for tap in range(taps - 2):
+        new_conv[tap] = conv_state[tap + 1]
+    new_conv[taps - 2] = branch_x
     block = recur_weight.shape[1]
     recur, inject = [], []
     for b in range(recur_weight.shape[0]):
@@ -187,6 +245,11 @@
     new_state_ref[...] = new_state
     mix_all[0] = (new_state * jax.nn.gelu(branch_g)).astype(BF16)
 
+    outs = [
+        pltpu.make_async_copy(new_state_ref, new_state_hbm, o_sem.at[0]),
+        pltpu.make_async_copy(new_conv, new_conv_hbm, o_sem.at[1]),
+        pltpu.make_async_copy(result, result_hbm, o_sem.at[2]),
+    ]
     mix_copies = []
     for number, member in enumerate(peers):
         mix_copies.append(
@@ -199,9 +262,11 @@
             )
         )
         mix_copies[-1].start()
+    outs[0].start()
+    outs[1].start()
     target = lax.broadcasted_iota(jnp.int32, (experts * slots, rows), 0)
     dispatch = jnp.where((target == slot_r0) | (target == slot_r1), 1.0, 0.0).astype(BF16)
-    copies[2].wait()
+    copies[16].wait()
     mixed = tokens[...].astype(F32)
     for number, member in enumerate((t,) + peers):
         if number:
@@ -265,9 +330,8 @@
 
     lax.fori_loop(0, chunks + 1, spread, 0)
 
-    for number in (3, 4, 5):
+    for number in range(17, 21):
         copies[number].wait()
-    hidden_width = w_down.shape[0]
 
     def p_copy(j):
         return pltpu.make_async_remote_copy(
@@ -368,12 +432,16 @@
     lax.fori_loop(1, experts, gather, 0)
     result[...] = (
         stream_ref[...].astype(F32)
-        + route_weight[:, 0:1] * picked[:rows]
-        + route_weight[:, 1:2] * picked[rows:]
+        + weight_0 * picked[:rows]
+        + weight_1 * picked[rows:]
     ).astype(BF16)
+
+    outs[2].start()
 
     for copy in tok_copies + mix_copies:
         copy.wait_send()
+    for copy in outs:
+        copy.wait()
 
     def drain_ep(k, carry):
         ep_copy(k).wait_send()
@@ -425,20 +493,36 @@
     capacity = max(2, min((rows - 2) * top_count // PER_GROUP, 2 * rows * top_count // experts))
     slots = -(-capacity // 8) * 8
     chunks = experts // GROUP
-    conv_pre = conv_bias + jnp.sum(conv_state.astype(F32) * conv_taps[None, :-1], axis=1)
-    vmem = pl.BlockSpec(memory_space=pltpu.VMEM)
     anywhere = pl.BlockSpec(memory_space=pl.ANY)
     dma = pltpu.SemaphoreType.DMA
-    result, new_state, branch_x = pl.pallas_call(
+    result, new_state, new_conv = pl.pallas_call(
         functools.partial(kernel, experts, slots),
         out_shape=(
             jax.ShapeDtypeStruct((rows, quarter), BF16),
             jax.ShapeDtypeStruct((rows, chan), F32),
-            jax.ShapeDtypeStruct((rows, chan), BF16),
+            jax.ShapeDtypeStruct((conv_taps.shape[0] - 1, rows, chan), BF16),
         ),
-        in_specs=[vmem] * 15 + [anywhere] * 6,
-        out_specs=(vmem, vmem, vmem),
+        in_specs=[anywhere] * 21,
+        out_specs=(anywhere, anywhere, anywhere),
         scratch_shapes=[
+            pltpu.VMEM((rows, quarter), BF16),
+            pltpu.VMEM((1, width), F32),
+            pltpu.VMEM((top_count, rows), jnp.int32),
+            pltpu.VMEM((top_count, rows), F32),
+            pltpu.VMEM((1, rows), F32),
+            pltpu.VMEM((conv_taps.shape[0] - 1, rows, chan), BF16),
+            pltpu.VMEM(conv_taps.shape, F32),
+            pltpu.VMEM((1, chan), F32),
+            pltpu.VMEM(recur_weight.shape, BF16),
+            pltpu.VMEM((1, chan), F32),
+            pltpu.VMEM(inject_weight.shape, BF16),
+            pltpu.VMEM((1, chan), F32),
+            pltpu.VMEM((1, chan), F32),
+            pltpu.VMEM((rows, chan), F32),
+            pltpu.VMEM((1, width), F32),
+            pltpu.VMEM((rows, quarter), BF16),
+            pltpu.VMEM((rows, chan), F32),
+            pltpu.VMEM((conv_taps.shape[0] - 1, rows, chan), BF16),
             pltpu.VMEM((width, 2 * chan), BF16),
             pltpu.VMEM((output_weight.shape[0], quarter), BF16),
             pltpu.VMEM((width, 2 * hidden), BF16),
@@ -457,7 +541,8 @@
             pltpu.VMEM((experts, slots, quarter), BF16),
             pltpu.VMEM((experts, slots, quarter), BF16),
             pltpu.VMEM((2 * rows, quarter), F32),
-            dma((6,)),
+            dma((21,)),
+            dma((3,)),
             dma((3,)),
             dma((3,)),
             dma((3,)),
@@ -476,29 +561,28 @@
         compiler_params=pltpu.CompilerParams(collective_id=0, has_side_effects=True),
     )(
         tokens,
-        conv_pre,
-        lru_state,
         mix_gain[None],
-        conv_taps[-1:],
+        route_ids.T,
+        route_logits.T,
+        group_weight[None],
+        input_weight,
+        branch_weight,
+        conv_state.transpose(1, 0, 2),
+        conv_taps,
+        conv_bias[None],
         recur_weight,
         recur_bias[None],
         inject_weight,
         inject_bias[None],
         decay_param[None],
+        lru_state,
+        output_weight,
         moe_gain[None],
-        route_ids,
-        route_ids.T,
-        route_logits,
-        group_weight[:, None],
-        input_weight,
-        branch_weight,
-        output_weight,
         expert_gate,
         expert_up,
         expert_down,
     )
-    new_conv = jnp.concatenate([conv_state[:, 1:], branch_x[:, None, :]], axis=1)
-    return (result, new_state, new_conv)
+    return (result, new_state, new_conv.transpose(1, 0, 2))
 
 
 def solution(mesh):

time: 51.8 us -> 43.9 us (0.85)
  local copies, waits for them, and re-layouts: 8.44 us -> 2.97 us
  other arithmetic: 1.28 us -> 0 us
  Pallas kernels: 40.9 us -> 40 us
    slice x3 -> x0, local copies, waits for them, and re-layouts: 2.09 us -> none  [the longest x1 1.3 us: body(): conv_taps[-1:]]
    unnamed x16 -> x7, local copies, waits for them, and re-layouts: 5.02 us -> 2.97 us
    broadcast_in_dim x1 -> x0, local copies, waits for them, and re-layouts: 1.34 us -> none  [body(): group_weight[:, None]]
    pallas_call x1, Pallas kernels: 40.9 us -> 40 us  [body(): pl.pallas_call(functools.partial(kernel, experts, slots), out_shape=(jax....]
    concatenate x1 -> x0, other arithmetic: 0.64 us -> none  [body(): jnp.concatenate([conv_state[:, 1:], branch_x[:, None, :]], axis=1)]
    add x1 -> x0, other arithmetic: 0.62 us -> none  [body(): conv_bias + jnp.sum(conv_state.astype(F32) * conv_taps[None, :-1], axis=1)]
where the time goes in v2:
time: 43.9 us; the launch traced here: 43.7 us
  Pallas kernels  40 us (91%)
  local copies, waits for them, and re-layouts  2.97 us (7%)
  between operations  0.66 us (2%)
    pallas_call x1, Pallas kernels, body(): pl.pallas_call(functools.partial(kernel, experts, slots), out_shape=(jax....  40 us
    unnamed x7, local copies, waits for them, and re-layouts  2.97 us

profile of v2, /device:TPU:0, one launch (start us, length us, event | category | flops | bytes accessed | tf_op | source)
XLA Modules:
  0.0 43.7 jit_solution(2456329663685042475)
XLA Ops:
  0.6 40.0 %shard_map.220 = (bf16[48,512]{1,0:T(8,128)(2,1)}, f32[48,256]{1,0:T(8,128)}, bf16[3,48,256]{2,1,0:T(8,128)(2,1)}) custom-call(bf16[48,512]{1,0:T(8,128)(2,1)} %refs_0_.1, f32[1,2048]{1,0:T(1,128)} %bitcast.13, s32[2,48]{1,0:T(2,128)} %bitcast.15, f32[2,48]{1,0:T(2,128)} %bitcast.16, f32[1,48]{1,0:T(1,128)} %bitcast.21, bf16[2048,256]{1,0:T(8,128)(2,1)} %refs_5_.1, ...), custom_call_target="tpu_custom_call" | custom-call | tf_op jit(solution)/shard_map/pallas_call | solution.py:498
  40.7 0.0 copy-start.1
  40.7 1.4 %copy.27 = bf16[48,512]{1,0:T(8,128)(2,1)} copy(bf16[48,512]{1,0:T(8,128)(2,1)} %get-tuple-element.12) | data formatting | bytes 98304
  42.1 0.0 copy-done.1
  42.1 0.0 copy-start
  42.1 0.6 %copy.28 = f32[48,256]{1,0:T(8,128)} copy(f32[48,256]{1,0:T(8,128)S(1)} %copy-done.1) | data formatting | bytes 98304
  42.8 0.3 copy-done
  43.0 0.6 %copy.29 = bf16[48,3,256]{2,0,1:T(8,128)(2,1)} copy(bf16[48,3,256]{2,0,1:T(8,128)(2,1)S(1)} %bitcast.11) | data formatting | bytes 147456
Async XLA Ops:
  40.7 1.4 %copy-start.1 = (f32[48,256]{1,0:T(8,128)S(1)}, f32[48,256]{1,0:T(8,128)}, u32[]{:S(2)}) copy-start(f32[48,256]{1,0:T(8,128)} %get-tuple-element.13) | copy-start | bytes 147460
  42.1 0.9 %copy-start = (bf16[3,48,256]{2,1,0:T(8,128)(2,1)S(1)}, bf16[3,48,256]{2,1,0:T(8,128)(2,1)}, u32[]{:S(2)}) copy-start(bf16[3,48,256]{2,1,0:T(8,128)(2,1)} %get-tuple-element.8) | copy-start | bytes 221188

commit v3 on v2

--- a/solution.py
+++ b/solution.py
@@ -46,9 +46,9 @@
         gate_hbm,
         up_hbm,
         down_hbm,
-        result_hbm,
-        new_state_hbm,
-        new_conv_hbm,
+        result,
+        new_state_ref,
+        new_conv,
     ) = refs[:24]
     (
         tokens,
@@ -66,10 +66,7 @@
         decay_param,
         lru_state,
         moe_gain,
-        result,
-        new_state_ref,
-        new_conv,
-    ) = refs[24:42]
+    ) = refs[24:39]
     (
         w_in,
         w_out,
@@ -90,7 +87,6 @@
         rin,
         picked,
         w_sem,
-        o_sem,
         tok_send,
         tok_recv,
         mix_send,
@@ -105,7 +101,7 @@
         x_recv,
         r_send,
         r_recv,
-    ) = refs[42:]
+    ) = refs[39:]
     e = lax.axis_index("ep")
     t = lax.axis_index("tp")
     rows, quarter = tokens.shape
@@ -245,11 +241,6 @@
     new_state_ref[...] = new_state
     mix_all[0] = (new_state * jax.nn.gelu(branch_g)).astype(BF16)
 
-    outs = [
-        pltpu.make_async_copy(new_state_ref, new_state_hbm, o_sem.at[0]),
-        pltpu.make_async_copy(new_conv, new_conv_hbm, o_sem.at[1]),
-        pltpu.make_async_copy(result, result_hbm, o_sem.at[2]),
-    ]
     mix_copies = []
     for number, member in enumerate(peers):
         mix_copies.append(
@@ -262,8 +253,6 @@
             )
         )
         mix_copies[-1].start()
-    outs[0].start()
-    outs[1].start()
     target = lax.broadcasted_iota(jnp.int32, (experts * slots, rows), 0)
     dispatch = jnp.where((target == slot_r0) | (target == slot_r1), 1.0, 0.0).astype(BF16)
     copies[16].wait()
@@ -291,7 +280,7 @@
         )
 
     def ep_start(k, carry):
-        ep_copy(k).start()
+        ep_copy(experts - k).start()
         return carry
 
     lax.fori_loop(1, experts, ep_start, 0)
@@ -308,27 +297,25 @@
             device_id=there(member),
         )
 
-    def spread(j, carry):
+    last = chunks - 1
+
+    def spread(j):
         @pl.when(j < chunks)
         def _():
             for g in range(GROUP):
-                k = j * GROUP + g
+                k = (last - j) * GROUP + g
 
                 @pl.when(k > 0)
                 def _():
                     ep_copy(k).wait_recv()
 
-            forward(0, j).start()
-            forward(1, j).start()
-
-        @pl.when(j > 0)
+            forward(0, last - j).start()
+            forward(1, last - j).start()
+
+        @pl.when((j > 0) & (j <= chunks))
         def _():
-            forward(1, j - 1).wait_recv()
-            forward(2, j - 1).start()
-
-        return carry
-
-    lax.fori_loop(0, chunks + 1, spread, 0)
+            forward(1, last - j + 1).wait_recv()
+            forward(2, last - j + 1).start()
 
     for number in range(17, 21):
         copies[number].wait()
@@ -361,16 +348,20 @@
             device_id={"ep": to},
         )
 
-    def expert(j, carry):
-        @pl.when(j < chunks)
+    def expert(step, carry):
+        spread(step)
+        j = step - 2
+
+        @pl.when((j >= 0) & (j < chunks))
         def _():
-            forward(0, j).wait_recv()
-            forward(2, j).wait_recv()
+            b = last - j
+            forward(0, b).wait_recv()
+            forward(2, b).wait_recv()
             act = jnp.zeros((GROUP * slots, 2 * hidden_width), F32)
             sq = jnp.zeros((GROUP * slots, 1), F32)
             for member in range(4):
                 wide = jnp.concatenate(
-                    [arrived[member, j * GROUP + g].astype(F32) for g in range(GROUP)], axis=0
+                    [arrived[member, b * GROUP + g].astype(F32) for g in range(GROUP)], axis=0
                 )
                 span = pl.ds(member * quarter, quarter)
                 sq += jnp.sum(wide * wide, axis=1, keepdims=True)
@@ -382,24 +373,26 @@
                 span = pl.ds(pl.multiple_of(member * quarter, quarter), quarter)
                 return dot(hidden, w_down[:, span])
 
-            pbox[j, 0] = partial_out(part).astype(BF16)
-            pbox[j, 1] = partial_out(diag).astype(BF16)
-            p_copy(j).start()
-            keep_own[j] = partial_out(t)
-            keep_cross[j] = partial_out(cross)
+            pbox[b, 0] = partial_out(part).astype(BF16)
+            pbox[b, 1] = partial_out(diag).astype(BF16)
+            p_copy(b).start()
+            keep_own[b] = partial_out(t)
+            keep_cross[b] = partial_out(cross)
 
         @pl.when((j > 0) & (j <= chunks))
         def _():
-            p_copy(j - 1).wait_recv()
-            xbox[j - 1] = (keep_cross[j - 1] + pin[j - 1, 1].astype(F32)).astype(BF16)
-            x_copy(j - 1).start()
-
-        @pl.when(j > 1)
+            b = last - j + 1
+            p_copy(b).wait_recv()
+            xbox[b] = (keep_cross[b] + pin[b, 1].astype(F32)).astype(BF16)
+            x_copy(b).start()
+
+        @pl.when(j > 2)
         def _():
-            x_copy(j - 2).wait_recv()
-            done = keep_own[j - 2] + pin[j - 2, 0].astype(F32) + xin[j - 2].astype(F32)
+            b = last - j + 3
+            x_copy(b).wait_recv()
+            done = keep_own[b] + pin[b, 0].astype(F32) + xin[b].astype(F32)
             for g in range(GROUP):
-                k = (j - 2) * GROUP + g
+                k = b * GROUP + g
                 rbox[k] = done[g * slots : (g + 1) * slots].astype(BF16)
 
                 @pl.when(k > 0)
@@ -408,7 +401,7 @@
 
         return carry
 
-    lax.fori_loop(0, chunks + 2, expert, 0)
+    lax.fori_loop(0, chunks + 5, expert, 0)
 
     lane = lax.broadcasted_iota(jnp.int32, (rows, slots), 1)
 
@@ -424,7 +417,8 @@
 
     picked[...] = dot(choose(0), rbox[0])
 
-    def gather(k, carry):
+    def gather(step, carry):
+        k = experts - step
         r_copy(k).wait_recv()
         picked[...] += dot(choose(k), rin[k])
         return carry
@@ -436,12 +430,9 @@
         + weight_1 * picked[rows:]
     ).astype(BF16)
 
-    outs[2].start()
 
     for copy in tok_copies + mix_copies:
         copy.wait_send()
-    for copy in outs:
-        copy.wait()
 
     def drain_ep(k, carry):
         ep_copy(k).wait_send()
@@ -493,17 +484,19 @@
     capacity = max(2, min((rows - 2) * top_count // PER_GROUP, 2 * rows * top_count // experts))
     slots = -(-capacity // 8) * 8
     chunks = experts // GROUP
+    vmem = pl.BlockSpec(memory_space=pltpu.VMEM)
     anywhere = pl.BlockSpec(memory_space=pl.ANY)
     dma = pltpu.SemaphoreType.DMA
-    result, new_state, new_conv = pl.pallas_call(
+    shapes = (
+        jax.ShapeDtypeStruct((rows, quarter), BF16),
+        jax.ShapeDtypeStruct((rows, chan), F32),
+        jax.ShapeDtypeStruct((conv_taps.shape[0] - 1, rows, chan), BF16),
+    )
+    made = pl.pallas_call(
         functools.partial(kernel, experts, slots),
-        out_shape=(
-            jax.ShapeDtypeStruct((rows, quarter), BF16),
-            jax.ShapeDtypeStruct((rows, chan), F32),
-            jax.ShapeDtypeStruct((conv_taps.shape[0] - 1, rows, chan), BF16),
-        ),
+        out_shape=tuple(pltpu.VMEM(s.shape, s.dtype) for s in shapes),
         in_specs=[anywhere] * 21,
-        out_specs=(anywhere, anywhere, anywhere),
+        out_specs=(vmem, vmem, vmem),
         scratch_shapes=[
             pltpu.VMEM((rows, quarter), BF16),
             pltpu.VMEM((1, width), F32),
@@ -520,9 +513,6 @@
             pltpu.VMEM((1, chan), F32),
             pltpu.VMEM((rows, chan), F32),
             pltpu.VMEM((1, width), F32),
-            pltpu.VMEM((rows, quarter), BF16),
-            pltpu.VMEM((rows, chan), F32),
-            pltpu.VMEM((conv_taps.shape[0] - 1, rows, chan), BF16),
             pltpu.VMEM((width, 2 * chan), BF16),
             pltpu.VMEM((output_weight.shape[0], quarter), BF16),
             pltpu.VMEM((width, 2 * hidden), BF16),
@@ -542,7 +532,6 @@
             pltpu.VMEM((experts, slots, quarter), BF16),
             pltpu.VMEM((2 * rows, quarter), F32),
             dma((21,)),
-            dma((3,)),
             dma((3,)),
             dma((3,)),
             dma((3,)),
@@ -582,6 +571,7 @@
         expert_up,
         expert_down,
     )
+    result, new_state, new_conv = made
     return (result, new_state, new_conv.transpose(1, 0, 2))
 
 

time: 43.9 us -> 39.1 us (0.89)
  Pallas kernels: 40 us -> 36.5 us
  local copies, waits for them, and re-layouts: 2.97 us -> 1.87 us
    pallas_call x1, Pallas kernels: 40 us -> 36.5 us  [body(): pl.pallas_call(functools.partial(kernel, experts, slots), out_shape=tuple...]
    unnamed x7 -> x3, local copies, waits for them, and re-layouts: 2.97 us -> 1.87 us
where the time goes in v3:
time: 39.1 us; the launch traced here: 39 us
  Pallas kernels  36.5 us (93%)
  local copies, waits for them, and re-layouts  1.87 us (5%)
  between operations  0.65 us (2%)
    pallas_call x1, Pallas kernels, body(): pl.pallas_call(functools.partial(kernel, experts, slots), out_shape=tuple...  36.5 us
    unnamed x3, local copies, waits for them, and re-layouts  1.87 us

profile of v3, /device:TPU:0, one launch (start us, length us, event | category | flops | bytes accessed | tf_op | source)
XLA Modules:
  0.0 39.0 jit_solution(3282009163705015837)
XLA Ops:
  0.6 36.5 %shard_map.220 = (bf16[48,512]{1,0:T(8,128)(2,1)S(1)}, f32[48,256]{1,0:T(8,128)S(1)}, bf16[3,48,256]{2,1,0:T(8,128)(2,1)S(1)}) custom-call(bf16[48,512]{1,0:T(8,128)(2,1)} %refs_0_.1, f32[1,2048]{1,0:T(1,128)} %bitcast.13, s32[2,48]{1,0:T(2,128)} %bitcast.15, f32[2,48]{1,0:T(2,128)} %bitcast.16, f32[1,48]{1,0:T(1,128)} %bitcast.21, ...), custom_call_target="tpu_custom_call" | custom-call | tf_op jit(solution)/shard_map/pallas_call | solution.py:495
  37.1 0.6 %copy.27 = bf16[48,512]{1,0:T(8,128)(2,1)} copy(bf16[48,512]{1,0:T(8,128)(2,1)S(1)} %get-tuple-element.9) | data formatting | bytes 98304
  37.7 0.6 %copy.28 = f32[48,256]{1,0:T(8,128)} copy(f32[48,256]{1,0:T(8,128)S(1)} %get-tuple-element.10) | data formatting | bytes 98304
  38.3 0.6 %copy.29 = bf16[48,3,256]{2,0,1:T(8,128)(2,1)} copy(bf16[48,3,256]{2,0,1:T(8,128)(2,1)S(1)} %bitcast.11) | data formatting | bytes 147456
